TPU v7x, 32 devices: a whole 2x2x4 slice. The times are simulated.
32 devices in a mesh: grp: 2 (over y), fs: 4 (over z), tp: 4 (over x, core).
Axes of the slice: x: 2, y: 2, z: 4, core: 2. Of those that a mesh axis runs over, the one named last changes fastest.
Arguments:
- tokens: bfloat16 [8, 384, 2048], P(('grp', 'fs'), None, 'tp'), parts along dimension 0, may hold values from -16 to 16
- norm_gain: float32 [2048], P('tp'), may hold values from 0.1 to 1.9
- in_weight: bfloat16 [2048, 1024], P('fs', 'tp'), may hold values from -0.125 to 0.125
- pool_weight: bfloat16 [8, 128, 128], P('tp'), may hold values from -0.5 to 0.5
- pool_scale: float32 [1024], P('tp'), may hold values from 0.1 to 1.9
- out_weight: bfloat16 [1024, 2048], P('fs', 'tp'), may hold values from -0.1875 to 0.1875
- ffn_gain: float32 [2048], P('tp'), may hold values from 0.1 to 1.9
- gate_weight: bfloat16 [2048, 5632], P('fs', 'tp'), may hold values from -0.125 to 0.125
- up_weight: bfloat16 [2048, 5632], P('fs', 'tp'), may hold values from -0.125 to 0.125
- down_weight: bfloat16 [5632, 2048], P('tp', 'fs'), may hold values from -0.078125 to 0.078125
Outputs:
- output: bfloat16 [8, 384, 2048], P(('grp', 'fs'), None, 'tp'), parts along dimension 0
There are 2 independent parts, one for each index of `grp`. A program takes and returns all parts, laid end to end along the dimension named above; an argument that names none is the same for every part. Nothing has to cross between parts.
All inputs are finite; a program needn't handle non-finite values.
Results may differ from a plain program's by a relative error of at most 0.009.
Values may be sent and summed in bfloat16 or wider, within the bound.
A program may use at most 64 MiB of HBM per device.

v0:
```python
import jax
import jax.numpy as jnp
from jax import lax
from jax.sharding import PartitionSpec as P

D = 2048
GD = 128


EPSILON = 0.05
HALVES = (1, 2, 4, 8)


def local(
    tokens,
    norm_gain,
    in_weight,
    pool_weight,
    pool_scale,
    out_weight,
    ffn_gain,
    gate_weight,
    up_weight,
    down_weight,
):
    seq_local, length, feat_local = tokens.shape
    stream = tokens.astype(jnp.float32)
    first_square = lax.psum(jnp.sum(stream * stream, axis=-1), "tp")
    normed = (stream * lax.rsqrt(first_square[..., None] / D + EPSILON) * norm_gain).astype(
        jnp.bfloat16
    )
    in_full = lax.all_gather(in_weight, "fs", axis=0, tiled=True)
    channels = in_full.shape[1]
    weight_rows = in_full
    pool_input = jnp.einsum(
        "slk,kc->slc",
        lax.all_gather(normed, "tp", axis=2, tiled=True),
        weight_rows,
        preferred_element_type=jnp.float32,
    ).astype(jnp.bfloat16)
    pool_float = pool_input.astype(jnp.float32)
    group_local = pool_weight.shape[0]
    group_ids = lax.axis_index("tp") * group_local + jnp.arange(channels) // GD
    selector = group_ids % 4
    running = jnp.concatenate(
        [jnp.zeros((seq_local, 1, channels), jnp.float32), jnp.cumsum(pool_float, axis=1)], axis=1
    )
    position = jnp.arange(length)
    window_mean = jnp.zeros_like(pool_float)
    for window_index, half_width in enumerate(HALVES):
        upper_sum = jnp.concatenate(
            [running[:, half_width:], jnp.repeat(running[:, -1:], half_width, axis=1)], axis=1
        )[:, :length]
        lower_sum = jnp.concatenate(
            [
                jnp.zeros((seq_local, half_width, channels), jnp.float32),
                running[:, : length + 1 - half_width],
            ],
            axis=1,
        )[:, :length]
        counts = (
            jnp.minimum(position + half_width, length) - jnp.maximum(position - half_width, 0)
        ).astype(jnp.float32)
        window_mean = jnp.where(
            selector == window_index, (upper_sum - lower_sum) / counts[:, None], window_mean
        )
    deviation = (window_mean - pool_float).astype(jnp.bfloat16)
    grouped = deviation.reshape(seq_local, length, group_local, GD)
    mapped = jnp.einsum("slgc,gcd->slgd", grouped, pool_weight, preferred_element_type=jnp.float32)
    pooled = (mapped.reshape(seq_local, length, channels) * pool_scale).astype(jnp.bfloat16)
    out_full = lax.all_gather(out_weight, "fs", axis=0, tiled=True)
    weight_rows = out_full
    mixed = stream + jnp.einsum(
        "jut,tx->jux",
        lax.all_gather(pooled, "tp", axis=2, tiled=True),
        weight_rows,
        preferred_element_type=jnp.float32,
    )
    second_square = lax.psum(jnp.sum(mixed * mixed, axis=-1), "tp")
    normed_two = (mixed * lax.rsqrt(second_square[..., None] / D + EPSILON) * ffn_gain).astype(
        jnp.bfloat16
    )
    features_full = lax.all_gather(normed_two, "tp", axis=2, tiled=True)
    gate_sum = jnp.einsum(
        "slk,kf->slf",
        features_full,
        lax.all_gather(gate_weight, "fs", axis=0, tiled=True),
        preferred_element_type=jnp.float32,
    )
    up_sum = jnp.einsum(
        "slk,kf->slf",
        features_full,
        lax.all_gather(up_weight, "fs", axis=0, tiled=True),
        preferred_element_type=jnp.float32,
    )
    hidden = (jax.nn.silu(gate_sum) * up_sum).astype(jnp.bfloat16)
    partial_value = jnp.einsum(
        "hor,rn->hon",
        hidden,
        lax.all_gather(down_weight, "fs", axis=1, tiled=True),
        preferred_element_type=jnp.float32,
    )
    summed = lax.psum_scatter(
        partial_value.astype(jnp.bfloat16), "tp", scatter_dimension=2, tiled=True
    ).astype(jnp.float32)
    return (mixed + summed).astype(jnp.bfloat16)


def solution(mesh):
    return jax.shard_map(
        local,
        mesh=mesh,
        in_specs=(
            P(("grp", "fs"), None, "tp"),
            P("tp"),
            P("fs", "tp"),
            P("tp", None, None),
            P("tp"),
            P("fs", "tp"),
            P("tp"),
            P("fs", "tp"),
            P("fs", "tp"),
            P("tp", "fs"),
        ),
        out_specs=P(("grp", "fs"), None, "tp"),
        check_vma=False,
    )
```

profile of v0, /device:TPU:0, one launch (start us, length us, event | category | flops | bytes accessed | tf_op | source)
XLA Modules:
  0.0 485.2 jit_solution(12671679941246397171)
XLA Ops:
  6.5 0.0 all-gather.10.cloned.1.call-start
  6.5 0.7 all-gather.10.cloned.1.call-update
  7.3 0.0 all-gather.8.cloned.1.call-start
  7.3 1.2 fusion.17
  8.5 8.4 %psum.14 = f32[1,384]{1,0:T(1,128)S(1)} all-reduce(f32[1,384]{1,0:T(1,128)S(1)} %reduce_sum.23), channel_id=1, replica_groups=mesh['grp'=2,'fs'=4,'tp'=4] {'tp'}, use_global_device_ids=true, to_apply=%region_1.0 | all-reduce | flops 384 | bytes 3072 | tf_op jit(solution)/shard_map/psum | solution.py:28
  16.9 1.9 fusion.19
  18.8 0.0 all-gather.8.cloned.1.call-update
  18.8 0.0 all-gather.12.cloned.1.call-start
  18.8 0.7 all-gather.12.cloned.1.call-update
  19.5 0.0 all-gather.14.cloned.1.call-start
  19.6 20.0 %all-gather.10.cloned.1.call-done = bf16[2048,256]{1,0:T(8,128)(2,1)} async-done(((bf16[512,256]{1,0:T(8,128)(2,1)}), bf16[2048,256]{1,0:T(8,128)(2,1)}) %all-gather.10.cloned.1.call-update) | async-done | bytes 1048592 | tf_op jit(solution)/shard_map/all_gather | solution.py:32
  39.6 20.6 %all-gather.8.cloned.1.call-done = bf16[1,384,2048]{2,1,0:T(8,128)(2,1)} async-done(((bf16[1,384,512]{2,1,0:T(8,128)(2,1)}), bf16[1,384,2048]{2,1,0:T(8,128)(2,1)}) %all-gather.8.cloned.1.call-update) | async-done | bytes 1572880 | tf_op jit(solution)/shard_map/all_gather | solution.py:37
  60.2 2.3 fusion.14
  62.5 0.3 fusion.23
  62.8 0.1 copy.12
  63.0 0.1 fusion.63
  63.1 0.1 fusion.61
  63.1 0.1 fusion.62
  63.2 0.0 copy-start.3
  63.3 0.5 fusion.39
  63.8 0.0 copy-start.1
  63.8 0.1 reshape.225
  63.8 0.3 fusion.40
  64.1 0.1 fusion.38
  64.2 0.0 copy-start.2
  64.2 8.6 %all_gather.26 = bf16[1,384,1024]{1,2,0:T(8,128)(2,1)S(1)} all-gather(bf16[1,384,256]{1,2,0:T(8,128)(2,1)S(1)} %fusion.38), channel_id=1, replica_groups=mesh['grp'=2,'fs'=4,'tp'=4] {'tp'}, dimensions={2}, use_global_device_ids=true | all-gather | bytes 983040 | tf_op jit(solution)/shard_map/all_gather | solution.py:75
  72.8 17.0 %all-gather.12.cloned.1.call-done = bf16[1024,512]{1,0:T(8,128)(2,1)} async-done(((bf16[256,512]{1,0:T(8,128)(2,1)}), bf16[1024,512]{1,0:T(8,128)(2,1)}) %all-gather.12.cloned.1.call-update) | async-done | bytes 1048592 | tf_op jit(solution)/shard_map/all_gather | solution.py:71
  89.8 0.0 copy-done.1
  89.8 1.9 multiply_reduce_fusion
  91.8 6.1 %psum.15 = f32[1,384]{1,0:T(1,128)S(1)} all-reduce(f32[1,384]{1,0:T(1,128)S(1)} %reduce_sum.25), channel_id=1, replica_groups=mesh['grp'=2,'fs'=4,'tp'=4] {'tp'}, use_global_device_ids=true, to_apply=%region_5.6 | all-reduce | flops 384 | bytes 3072 | tf_op jit(solution)/shard_map/psum | solution.py:79
  97.9 0.9 multiply_convert_fusion
  98.8 0.0 all-gather.14.cloned.1.call-update
  98.8 0.0 all-gather.16.cloned.1.call-start
  98.8 0.5 all-gather.16.cloned.1.call-update
  99.4 0.0 all-gather.18.cloned.1.call-start
  99.4 0.5 all-gather.18.cloned.1.call-update
  99.9 0.0 all-gather.20.cloned.1.call-start
  100.0 0.7 all-gather.20.cloned.1.call-update
  100.7 0.0 reduce-scatter.2.cloned.1.call-start
  100.7 17.0 %all-gather.14.cloned.1.call-done = bf16[1,384,2048]{2,1,0:T(8,128)(2,1)} async-done(((bf16[1,384,512]{2,1,0:T(8,128)(2,1)}), bf16[1,384,2048]{2,1,0:T(8,128)(2,1)}) %all-gather.14.cloned.1.call-update) | async-done | bytes 1572880 | tf_op jit(solution)/shard_map/all_gather | solution.py:83
  117.8 108.1 %all-gather.16.cloned.1.call-done = bf16[2048,1408]{1,0:T(8,128)(2,1)} async-done(((bf16[512,1408]{1,0:T(8,128)(2,1)}), bf16[2048,1408]{1,0:T(8,128)(2,1)}) %all-gather.16.cloned.1.call-update) | async-done | bytes 5767184 | tf_op jit(solution)/shard_map/all_gather | solution.py:87
  225.9 7.1 %fusion.3 = f32[384,1408]{1,0:T(8,128)} fusion(bf16[2048,1408]{1,0:T(8,128)(2,1)} %all-gather.16.cloned.1.call-done, bf16[1,384,2048]{2,1,0:T(8,128)(2,1)} %all-gather.14.cloned.1.call-done), kind=kOutput, calls=%fused_computation.5 | convolution fusion | flops 2214592512 | bytes 9502720 | tf_op jit(solution)/shard_map/slk,kf->slf/dot_general | solution.py:84
  233.0 99.3 %all-gather.18.cloned.1.call-done = bf16[2048,1408]{1,0:T(8,128)(2,1)} async-done(((bf16[512,1408]{1,0:T(8,128)(2,1)}), bf16[2048,1408]{1,0:T(8,128)(2,1)}) %all-gather.18.cloned.1.call-update) | async-done | bytes 5767184 | tf_op jit(solution)/shard_map/all_gather | solution.py:93
  332.3 106.5 %all-gather.20.cloned.1.call-done = bf16[1408,2048]{1,0:T(8,128)(2,1)} async-done(((bf16[1408,512]{1,0:T(8,128)(2,1)}), bf16[1408,2048]{1,0:T(8,128)(2,1)}) %all-gather.20.cloned.1.call-update) | async-done | bytes 5767184 | tf_op jit(solution)/shard_map/all_gather | solution.py:100
  438.9 11.3 %fusion.1 = bf16[1,384,2048]{2,1,0:T(8,128)(2,1)} fusion(bf16[1408,2048]{1,0:T(8,128)(2,1)} %all-gather.20.cloned.1.call-done, bf16[2048,1408]{1,0:T(8,128)(2,1)} %all-gather.18.cloned.1.call-done, f32[384,1408]{1,0:T(8,128)} %fusion.3, bf16[1,384,2048]{2,1,0:T(8,128)(2,1)S(1)} %copy-done.4), kind=kOutput, calls=%fused_computation.3 | convolution fusion | flops 4433215488 | bytes 16842752 | tf_op jit(solution)/shard_map/hor,rn->hon/dot_general | solution.py:97
  450.1 0.0 reduce-scatter.2.cloned.1.call-update
  450.2 26.4 %reduce-scatter.2.cloned.1.call-done = bf16[1,384,512]{2,1,0:T(8,128)(2,1)} async-done(((bf16[1,384,2048]{2,1,0:T(8,128)(2,1)}), bf16[1,384,512]{2,1,0:T(8,128)(2,1)}) %reduce-scatter.2.cloned.1.call-update) | async-done | bytes 393232 | tf_op jit(solution)/shard_map/reduce_scatter | solution.py:103
  476.5 1.9 add_convert_fusion
  (23 shorter events, 0.2 us)
Async XLA Ops:
  6.5 57.3 %copy-start = (bf16[2,128,128]{2,1,0:T(8,128)(2,1)S(1)}, bf16[2,128,128]{2,1,0:T(8,128)(2,1)}, u32[]{:S(2)}) copy-start(bf16[2,128,128]{2,1,0:T(8,128)(2,1)} %param.13) | copy-start | bytes 196612
  6.5 33.1 %all-gather.10.cloned.1.call-start = ((), (), s32[]{:S(2)}) async-start(), calls=%async_computation.2 | async-start | bytes 1310720 | tf_op jit(solution)/shard_map/all_gather | solution.py:32
  7.3 53.0 %all-gather.8.cloned.1.call-start = ((), (), s32[]{:S(2)}) async-start(), calls=%async_computation.1 | async-start | bytes 1966080 | tf_op jit(solution)/shard_map/all_gather | solution.py:37
  18.8 71.0 %all-gather.12.cloned.1.call-start = ((), (), s32[]{:S(2)}) async-start(), calls=%async_computation.3 | async-start | bytes 1310720 | tf_op jit(solution)/shard_map/all_gather | solution.py:71
  19.5 98.3 %all-gather.14.cloned.1.call-start = ((), (), s32[]{:S(2)}) async-start(), calls=%async_computation.4 | async-start | bytes 1966080 | tf_op jit(solution)/shard_map/all_gather | solution.py:83
  63.2 0.9 copy-start.3
  63.8 26.1 %copy-start.1 = (bf16[1,384,512]{2,1,0:T(8,128)(2,1)S(1)}, bf16[1,384,512]{2,1,0:T(8,128)(2,1)}, u32[]{:S(2)}) copy-start(bf16[1,384,512]{2,1,0:T(8,128)(2,1)} %param.10) | copy-start | bytes 1179652
  64.2 33.6 %copy-start.2 = (f32[512]{0:T(512)S(1)}, f32[512]{0:T(512)}, u32[]{:S(2)}) copy-start(f32[512]{0:T(512)} %param.16) | copy-start | bytes 6148
  98.8 127.2 %all-gather.16.cloned.1.call-start = ((), (), s32[]{:S(2)}) async-start(), calls=%async_computation.5 | async-start | bytes 7208960 | tf_op jit(solution)/shard_map/all_gather | solution.py:87
  99.4 233.0 %all-gather.18.cloned.1.call-start = ((), (), s32[]{:S(2)}) async-start(), calls=%async_computation.6 | async-start | bytes 7208960 | tf_op jit(solution)/shard_map/all_gather | solution.py:93
  99.9 338.9 %all-gather.20.cloned.1.call-start = ((), (), s32[]{:S(2)}) async-start(), calls=%async_computation.7 | async-start | bytes 7208960 | tf_op jit(solution)/shard_map/all_gather | solution.py:100
  100.7 375.8 %reduce-scatter.2.cloned.1.call-start = ((), (), s32[]{:S(2)}) async-start(), calls=%async_computation.8 | async-start | bytes 1966080 | tf_op jit(solution)/shard_map/reduce_scatter | solution.py:103
  117.8 321.1 %copy-start.4 = (bf16[1,384,2048]{2,1,0:T(8,128)(2,1)S(1)}, bf16[1,384,2048]{2,1,0:T(8,128)(2,1)}, u32[]{:S(2)}) copy-start(bf16[1,384,2048]{2,1,0:T(8,128)(2,1)} %all-gather.14.cloned.1.call-done) | copy-start | bytes 4718596
Sparse Core Ops, SparseCore 0:
  8.9 30.6 all-gather.9
  41.2 18.9 all-gather.7
  61.8 27.9 all-gather.11
  98.9 18.8 all-gather.13
  119.2 106.6 all-gather.15
  227.4 104.9 all-gather.17
  333.9 104.9 all-gather.19
  450.3 26.2 reduce-scatter.1
where the time goes:
time: 486 us; the launch traced here: 485 us
  waiting for transfers between devices  418 us (86%)
  blocking collectives  23 us (5%)
  matrix products  22.8 us (5%)
  between operations  13.7 us (3%)
  other arithmetic  6.86 us (1%)
    all_gather x1, waiting for transfers between devices, local(): lax.all_gather(gate_weight, 'fs', axis=0, tiled=True)  108 us
    all_gather x1, waiting for transfers between devices, local(): lax.all_gather(down_weight, 'fs', axis=1, tiled=True)  107 us
    all_gather x1, waiting for transfers between devices, local(): lax.all_gather(up_weight, 'fs', axis=0, tiled=True)  99.3 us
    reduce_scatter x1, waiting for transfers between devices, local(): lax.psum_scatter(partial_value.astype(jnp.bfloat16), 'tp', scatter_dimens...  26.4 us
    all_gather x1, waiting for transfers between devices, local(): lax.all_gather(normed, 'tp', axis=2, tiled=True)  20.6 us
    all_gather x1, waiting for transfers between devices, local(): in_full = lax.all_gather(in_weight, 'fs', axis=0, tiled=True)  20 us
    all_gather x1, waiting for transfers between devices, local(): features_full = lax.all_gather(normed_two, 'tp', axis=2, tiled=True)  17 us
    all_gather x1, waiting for transfers between devices, local(): out_full = lax.all_gather(out_weight, 'fs', axis=0, tiled=True)  17 us
  transfers between devices with their start and end apart: 8, of which 8 were waited for; matrix products, arithmetic and copies ran while one was open for 3% of the time, Pallas kernels for 0%

commit v1 on v0

--- a/solution.py
+++ b/solution.py
@@ -1,6 +1,10 @@
+import functools
+
 import jax
 import jax.numpy as jnp
 from jax import lax
+from jax.experimental import pallas as pl
+from jax.experimental.pallas import tpu as pltpu
 from jax.sharding import PartitionSpec as P
 
 D = 2048
@@ -106,9 +110,422 @@
     return (mixed + summed).astype(jnp.bfloat16)
 
 
+SPLITS = (1, 1, 2, 2, 4)
+W_IN, W_OUT, W_GATE, W_UP, W_DOWN = range(5)
+FIRST = tuple(sum(SPLITS[:k]) for k in range(5))
+E_TOK, E_GAIN, E_POOL, E_SQ, E_X2, E_RS = range(6)
+MESH = pl.DeviceIdType.MESH
+
+
+def kernel(
+    n_fs,
+    n_tp,
+    tokens,
+    gain1,
+    pool_w,
+    scale,
+    gain2,
+    w_in,
+    w_out,
+    w_gate,
+    w_up,
+    w_down,
+    out,
+    b_in,
+    b_out,
+    b_gate,
+    b_up,
+    b_down,
+    tok,
+    gain_all,
+    pooled,
+    sq,
+    x2,
+    mixed,
+    gate_acc,
+    hidden,
+    part,
+    rs,
+    stage,
+    z_recv,
+    y_recv,
+    r_send,
+    l_send,
+    y_send,
+    own_sem,
+    e_send,
+    e_recv,
+):
+    g, i, j = lax.axis_index("grp"), lax.axis_index("fs"), lax.axis_index("tp")
+    length, feat = tokens.shape
+    bufs = (b_in, b_out, b_gate, b_up, b_down)
+    srcs = (w_in, w_out, w_gate, w_up, w_down)
+    has_left, has_right = i > 0, i < n_fs - 1
+
+    barrier = pltpu.get_barrier_semaphore()
+
+    def greet(device):
+        pl.semaphore_signal(barrier, inc=1, device_id=device, device_id_type=MESH)
+
+    pl.when(has_left)(lambda: greet({"fs": i - 1}))
+    pl.when(has_right)(lambda: greet({"fs": i + 1}))
+    greet({"grp": 1 - g})
+    for o in range(1, n_tp):
+        greet({"tp": lax.rem(j + o, n_tp)})
+    pl.semaphore_wait(barrier, n_tp + jnp.minimum(i, 1) + jnp.minimum(n_fs - 1 - i, 1))
+
+    def rows(k):
+        return srcs[k].shape[0]
+
+    def slot(k, s, half, q):
+        step = rows(k) // 2 // SPLITS[k]
+        off = pl.multiple_of(s * rows(k) + half * (rows(k) // 2) + q * step, 16)
+        return bufs[k].at[pl.ds(off, step)]
+
+    def own_rows(k, q):
+        step = rows(k) // 2 // SPLITS[k]
+        return srcs[k].at[pl.ds(pl.multiple_of(g * (rows(k) // 2) + q * step, 16), step)]
+
+    def z_copy(k, q, s, right, own):
+        item = FIRST[k] + q
+        return pltpu.make_async_remote_copy(
+            src_ref=own_rows(k, q) if own else slot(k, s, g, q),
+            dst_ref=slot(k, s, g, q),
+            send_sem=(r_send if right else l_send).at[item, s],
+            recv_sem=z_recv.at[item, s],
+            device_id={"fs": i + 1 if right else i - 1},
+            device_id_type=MESH,
+        )
+
+    def y_copy(k, q, s, half):
+        item = FIRST[k] + q
+        return pltpu.make_async_remote_copy(
+            src_ref=slot(k, s, half, q),
+            dst_ref=slot(k, s, half, q),
+            send_sem=y_send.at[item, s],
+            recv_sem=y_recv.at[item, s],
+            device_id={"grp": 1 - g},
+            device_id_type=MESH,
+        )
+
+    def send_own(k):
+        for q in range(SPLITS[k]):
+            pl.when(has_right)(lambda q=q: z_copy(k, q, i, True, True).start())
+            pl.when(has_left)(lambda q=q: z_copy(k, q, i, False, True).start())
+
+    def serve(k, d, q):
+        @pl.when(i - d >= 0)
+        def _():
+            s = i - d
+            z_copy(k, q, s, True, False).wait_recv()
+            pl.when(has_right)(lambda: z_copy(k, q, s, True, False).start())
+            y_copy(k, q, s, g).start()
+
+        @pl.when(i + d < n_fs)
+        def _():
+            s = i + d
+            z_copy(k, q, s, False, False).wait_recv()
+            pl.when(has_left)(lambda: z_copy(k, q, s, False, False).start())
+            y_copy(k, q, s, g).start()
+
+    def serve_all(k, d):
+        for q in range(SPLITS[k]):
+            serve(k, d, q)
+
+    def each(d, f):
+        pl.when(i - d >= 0)(lambda: f(i - d))
+        pl.when(i + d < n_fs)(lambda: f(i + d))
+
+    def wait_y(k, s):
+        for q in range(SPLITS[k]):
+            y_copy(k, q, s, 1 - g).wait_recv()
+
+    def own_copy(k):
+        off = pl.multiple_of(i * rows(k), 16)
+        return pltpu.make_async_copy(srcs[k], bufs[k].at[pl.ds(off, rows(k))], own_sem.at[k])
+
+    def arrived(k):
+        own_copy(k).wait()
+        for d in range(1, n_fs):
+            each(d, lambda s: wait_y(k, s))
+
+    def cols(ref, t, width):
+        return ref.at[:, pl.ds(pl.multiple_of(t * width, 128), width)]
+
+    def e_copy(e, o, src, dst):
+        return pltpu.make_async_remote_copy(
+            src_ref=src,
+            dst_ref=dst(j),
+            send_sem=e_send.at[e, o],
+            recv_sem=e_recv.at[e, j],
+            device_id={"tp": lax.rem(j + o, n_tp)},
+            device_id_type=MESH,
+        )
+
+    def share(e, src, dst):
+        for o in range(1, n_tp):
+            e_copy(e, o, src, dst).start()
+
+    def take(e, src, dst):
+        for o in range(1, n_tp):
+            p = lax.rem(j + o, n_tp)
+            pltpu.make_async_remote_copy(
+                src_ref=src,
+                dst_ref=dst(p),
+                send_sem=e_send.at[e, o],
+                recv_sem=e_recv.at[e, p],
+                device_id={"tp": p},
+                device_id_type=MESH,
+            ).wait_recv()
+
+    channels = w_in.shape[1]
+    tok_at = lambda t: cols(tok, t, feat)
+    gain_at = lambda t: cols(gain_all, t, feat)
+    pool_at = lambda t: cols(pooled, t, channels)
+    sq_at = lambda t: sq.at[t]
+    x2_at = lambda t: cols(x2, t, feat)
+
+    send_own(W_IN)
+    send_own(W_OUT)
+    share(E_TOK, tokens, tok_at)
+    share(E_GAIN, gain1, gain_at)
+    for k in range(5):
+        own_copy(k).start()
+    cols(tok, j, feat)[...] = tokens[...]
+    cols(gain_all, j, feat)[...] = gain1[...]
+    for d in range(1, n_fs):
+        serve_all(W_IN, d)
+        serve_all(W_OUT, d)
+    send_own(W_GATE)
+    send_own(W_UP)
+
+    take(E_TOK, tokens, tok_at)
+    take(E_GAIN, gain1, gain_at)
+    width = tok.shape[1]
+    block = 32
+    @pl.loop(0, length // block)
+    def _(r):
+        at = pl.ds(pl.multiple_of(r * block, block), block)
+        x = tok[at, :].astype(jnp.float32)
+        square = jnp.sum(x * x, axis=-1, keepdims=True)
+        x2[at, :] = (x * lax.rsqrt(square / width + EPSILON) * gain_all[0:1, :]).astype(
+            jnp.bfloat16
+        )
+
+    arrived(W_IN)
+    pool_in = jnp.dot(x2[...], b_in[...], preferred_element_type=jnp.float32).astype(jnp.bfloat16)
+    group_local = pool_w.shape[0]
+    row = lax.broadcasted_iota(jnp.int32, (length, length), 0)
+    col = lax.broadcasted_iota(jnp.int32, (length, length), 1)
+    at_row = lax.broadcasted_iota(jnp.int32, (length, 128), 0)
+    for k in range(group_local):
+        level = lax.rem(j * group_local + k, len(HALVES))
+        half = jnp.int32(HALVES[0])
+        for index, value in enumerate(HALVES):
+            half = jnp.where(level == index, jnp.int32(value), half)
+        inside = (col >= row - half) & (col < row + half)
+        band = jnp.where(inside, 1.0, 0.0).astype(jnp.bfloat16)
+        count = jnp.minimum(at_row + half, length) - jnp.maximum(at_row - half, 0)
+        piece = pool_in[:, k * GD : (k + 1) * GD]
+        total = jnp.dot(band, piece, preferred_element_type=jnp.float32)
+        deviation = total / count[:, :1].astype(jnp.float32) - piece.astype(jnp.float32)
+        mapped = jnp.dot(
+            deviation.astype(jnp.bfloat16), pool_w[k], preferred_element_type=jnp.float32
+        )
+        stage[:, k * GD : (k + 1) * GD] = (
+            mapped * scale[0:1, k * GD : (k + 1) * GD]
+        ).astype(jnp.bfloat16)
+    own_pool = stage.at[:, pl.ds(0, channels)]
+    cols(pooled, j, channels)[...] = own_pool[...]
+    share(E_POOL, own_pool, pool_at)
+    serve_all(W_GATE, 1)
+    send_own(W_DOWN)
+    arrived(W_OUT)
+    take(E_POOL, own_pool, pool_at)
+    mixed[...] = tokens[...].astype(jnp.float32) + jnp.dot(
+        pooled[...], b_out[...], preferred_element_type=jnp.float32
+    )
+    partial_sq = jnp.zeros((length, 128), jnp.float32)
+    for c in range(feat // 128):
+        m = mixed[:, c * 128 : (c + 1) * 128]
+        partial_sq = partial_sq + m * m
+    own_sq = sq.at[n_tp]
+    own_sq[...] = partial_sq
+    share(E_SQ, own_sq, sq_at)
+    take(E_SQ, own_sq, sq_at)
+    total_sq = sq[n_tp]
+    for o in range(1, n_tp):
+        total_sq = total_sq + sq[lax.rem(j + o, n_tp)]
+    second = jnp.sum(total_sq, axis=-1, keepdims=True)
+    own_x2 = stage.at[:, pl.ds(channels, feat)]
+    own_x2[...] = (mixed[...] * lax.rsqrt(second / width + EPSILON) * gain2[0:1, :]).astype(
+        jnp.bfloat16
+    )
+    x2_full = tok
+    cols(x2_full, j, feat)[...] = own_x2[...]
+    x2_at = lambda t: cols(x2_full, t, feat)
+    share(E_X2, own_x2, x2_at)
+
+    for d in range(2, n_fs):
+        serve_all(W_GATE, d)
+    take(E_X2, own_x2, x2_at)
+    serve_all(W_UP, 1)
+    arrived(W_GATE)
+
+    def project(b, acc, at):
+        depth = 512 if width % 512 == 0 else 128
+        acc[...] = jnp.zeros_like(acc)
+
+        @pl.loop(0, width // depth)
+        def _(c):
+            k_at = pl.ds(pl.multiple_of(c * depth, depth), depth)
+            acc[...] += jnp.dot(at[:, k_at], b[k_at, :], preferred_element_type=jnp.float32)
+
+    project(b_gate, gate_acc, x2_full)
+    for d in range(2, n_fs):
+        serve_all(W_UP, d)
+    serve_all(W_DOWN, 1)
+    arrived(W_UP)
+    up_chunk = 64
+
+    @pl.loop(0, length // up_chunk)
+    def _(r):
+        at = pl.ds(pl.multiple_of(r * up_chunk, up_chunk), up_chunk)
+        up = jnp.dot(x2_full[at, :], b_up[...], preferred_element_type=jnp.float32)
+        gate = gate_acc[at, :]
+        hidden[at, :] = (gate / (1.0 + jnp.exp(-gate)) * up).astype(jnp.bfloat16)
+
+    def rs_copy(s):
+        return pltpu.make_async_remote_copy(
+            src_ref=part.at[s],
+            dst_ref=rs.at[j],
+            send_sem=e_send.at[E_RS, s],
+            recv_sem=e_recv.at[E_RS, j],
+            device_id={"tp": s},
+            device_id_type=MESH,
+        )
+
+    def down(s):
+        at = pl.ds(pl.multiple_of(s * rows(W_DOWN), 16), rows(W_DOWN))
+        part[s] = jnp.dot(
+            hidden[...], b_down[at, :], preferred_element_type=jnp.float32
+        ).astype(jnp.bfloat16)
+        pl.when(s != j)(lambda: rs_copy(s).start())
+
+    own_copy(W_DOWN).wait()
+    down(i)
+    for d in range(1, n_fs):
+        if d > 1:
+            serve_all(W_DOWN, d)
+
+        def finish(s):
+            wait_y(W_DOWN, s)
+            down(s)
+
+        each(d, finish)
+
+    for o in range(1, n_tp):
+        p = lax.rem(j + o, n_tp)
+        pltpu.make_async_remote_copy(
+            src_ref=part.at[p],
+            dst_ref=rs.at[p],
+            send_sem=e_send.at[E_RS, p],
+            recv_sem=e_recv.at[E_RS, p],
+            device_id={"tp": p},
+            device_id_type=MESH,
+        ).wait_recv()
+    summed = part[j].astype(jnp.float32)
+    for o in range(1, n_tp):
+        summed = summed + rs[lax.rem(j + o, n_tp)].astype(jnp.float32)
+    out[...] = (mixed[...] + summed).astype(jnp.bfloat16)
+
+    for k in range(5):
+        for q in range(SPLITS[k]):
+            pl.when(has_right)(lambda k=k, q=q: z_copy(k, q, i, True, True).wait_send())
+            pl.when(has_left)(lambda k=k, q=q: z_copy(k, q, i, False, True).wait_send())
+            for d in range(1, n_fs):
+
+                @pl.when(i - d >= 0)
+                def _(k=k, q=q, d=d):
+                    pl.when(has_right)(lambda: z_copy(k, q, i - d, True, False).wait_send())
+                    y_copy(k, q, i - d, g).wait_send()
+
+                @pl.when(i + d < n_fs)
+                def _(k=k, q=q, d=d):
+                    pl.when(has_left)(lambda: z_copy(k, q, i + d, False, False).wait_send())
+                    y_copy(k, q, i + d, g).wait_send()
+
+    for o in range(1, n_tp):
+        e_copy(E_TOK, o, tokens, tok_at).wait_send()
+        e_copy(E_GAIN, o, gain1, gain_at).wait_send()
+        e_copy(E_POOL, o, own_pool, pool_at).wait_send()
+        e_copy(E_SQ, o, own_sq, sq_at).wait_send()
+        e_copy(E_X2, o, own_x2, x2_at).wait_send()
+        rs_copy(lax.rem(j + o, n_tp)).wait_send()
+
+
+def fused(
+    n_fs,
+    n_tp,
+    tokens,
+    norm_gain,
+    in_weight,
+    pool_weight,
+    pool_scale,
+    out_weight,
+    ffn_gain,
+    gate_weight,
+    up_weight,
+    down_weight,
+):
+    _, length, feat = tokens.shape
+    channels, units = in_weight.shape[1], gate_weight.shape[1]
+    weights = (in_weight, out_weight, gate_weight, up_weight, down_weight)
+    wide = lambda v: jnp.broadcast_to(v, (8, v.shape[0]))
+    vmem = pl.BlockSpec(memory_space=pltpu.VMEM)
+    hbm = pl.BlockSpec(memory_space=pl.ANY)
+    items = sum(SPLITS)
+    bf16, f32 = jnp.bfloat16, jnp.float32
+    sems = pltpu.SemaphoreType.DMA
+    return pl.pallas_call(
+        functools.partial(kernel, n_fs, n_tp),
+        out_shape=jax.ShapeDtypeStruct((length, feat), bf16),
+        in_specs=[vmem] * 5 + [hbm] * 5,
+        out_specs=vmem,
+        scratch_shapes=[pltpu.VMEM((n_fs * w.shape[0], w.shape[1]), bf16) for w in weights]
+        + [
+            pltpu.VMEM((length, n_tp * feat), bf16),
+            pltpu.VMEM((8, n_tp * feat), f32),
+            pltpu.VMEM((length, n_tp * channels), bf16),
+            pltpu.VMEM((n_tp + 1, length, 128), f32),
+            pltpu.VMEM((length, n_tp * feat), bf16),
+            pltpu.VMEM((length, feat), f32),
+            pltpu.VMEM((length, units), f32),
+            pltpu.VMEM((length, units), bf16),
+            pltpu.VMEM((n_tp, length, feat), bf16),
+            pltpu.VMEM((n_tp, length, feat), bf16),
+            pltpu.VMEM((length, channels + feat), bf16),
+        ]
+        + [sems((items, n_fs))] * 5
+        + [sems((5,)), sems((6, n_tp)), sems((6, n_tp))],
+        compiler_params=pltpu.CompilerParams(
+            collective_id=0, has_side_effects=True, vmem_limit_bytes=56 * 1024 * 1024
+        ),
+    )(
+        tokens[0],
+        wide(norm_gain),
+        pool_weight,
+        wide(pool_scale),
+        wide(ffn_gain),
+        *weights,
+    )[None]
+
+
 def solution(mesh):
+    n_grp, n_fs, n_tp = mesh.shape["grp"], mesh.shape["fs"], mesh.shape["tp"]
+    body = functools.partial(fused, n_fs, n_tp) if n_grp == 2 and n_fs == n_tp <= 8 else local
     return jax.shard_map(
-        local,
+        body,
         mesh=mesh,
         in_specs=(
             P(("grp", "fs"), None, "tp"),

time: 486 us -> 218 us (0.45)
  waiting for transfers between devices: 418 us -> 0 us
  Pallas kernels: 0 us -> 212 us
  blocking collectives: 23 us -> 0 us
  matrix products: 22.8 us -> 0 us
  between operations: 13.7 us -> 0.01 us
  other arithmetic: 6.86 us -> 0 us
  local copies, waits for them, and re-layouts: 0.38 us -> 5.61 us
    all_gather x7 -> x0, waiting for transfers between devices: 389 us -> none  [the longest x1 108 us: local(): lax.all_gather(gate_weight, 'fs', axis=0, tiled=True)]
    pallas_call x0 -> x1, Pallas kernels: none -> 212 us  [fused(): pl.pallas_call(functools.partial(kernel, n_fs, n_tp), out_shape=jax.Shape...]
    reduce_scatter x1 -> x0, waiting for transfers between devices: 26.4 us -> none  [local(): lax.psum_scatter(partial_value.astype(jnp.bfloat16), 'tp', scatter_dimens...]
    dot_general x5 -> x0, matrix products: 22.8 us -> none  [the longest x1 11.3 us: local(): jnp.einsum('hor,rn->hon', hidden, lax.all_gather(down_weight, 'fs', axis=...]
    psum x2 -> x0, blocking collectives: 14.5 us -> none  [the longest x1 8.37 us: local(): first_square = lax.psum(jnp.sum(stream * stream, axis=-1), 'tp')]
    all_gather x1 -> x0, blocking collectives: 8.58 us -> none  [local(): lax.all_gather(pooled, 'tp', axis=2, tiled=True)]
    convert_element_type x7 -> x0, other arithmetic: 5.27 us -> none  [the longest x1 1.91 us: local(): (stream * lax.rsqrt(first_square[..., None] / D + EPSILON) * norm_gain).a...]
  transfers between devices with their start and end apart: 8 -> 0, of which waited for: 8 -> 0; matrix products, arithmetic and copies ran while one was open for 3% -> 0% of each run, Pallas kernels for 0% -> 0%
where the time goes in v1:
time: 218 us
  Pallas kernels  212 us (97%)
  local copies, waits for them, and re-layouts  5.61 us (3%)
    pallas_call x1, Pallas kernels, fused(): pl.pallas_call(functools.partial(kernel, n_fs, n_tp), out_shape=jax.Shape...  212 us

profile of v1, /device:TPU:0, one launch (start us, length us, event | category | flops | bytes accessed | tf_op | source)
XLA Modules:
  0.0 217.6 jit_solution(8582877267825241766)
XLA Ops:
  0.0 1.3 broadcast_in_dim.13.scale
  1.3 1.3 broadcast_in_dim.12.gain1
  2.6 1.3 broadcast_in_dim.14.gain2
  3.8 212.0 %shard_map.100 = bf16[384,512]{1,0:T(8,128)(2,1)} custom-call(bf16[384,512]{1,0:T(8,128)(2,1)} %bitcast.3, f32[8,512]{1,0:T(8,128)} %broadcast_in_dim.12.gain1, bf16[2,128,128]{2,1,0:T(8,128)(2,1)} %pool_w.1, f32[8,256]{1,0:T(8,128)} %broadcast_in_dim.13.scale, f32[8,512]{1,0:T(8,128)} %broadcast_in_dim.14.gain2, bf16[512,256]{1,0:T(8,128)(2,1)} %w_in.1, ...), custom_call_target="tpu_custom_call" | custom-call | tf_op jit(solution)/shard_map/pallas_call | solution.py:490
  215.9 1.8 copy.12

commit v2 on v1

--- a/solution.py
+++ b/solution.py
@@ -110,7 +110,7 @@
     return (mixed + summed).astype(jnp.bfloat16)
 
 
-SPLITS = (1, 1, 2, 2, 4)
+SPLITS = (1, 1, 4, 2, 4)
 W_IN, W_OUT, W_GATE, W_UP, W_DOWN = range(5)
 FIRST = tuple(sum(SPLITS[:k]) for k in range(5))
 E_TOK, E_GAIN, E_POOL, E_SQ, E_X2, E_RS = range(6)
@@ -208,8 +208,8 @@
             device_id_type=MESH,
         )
 
-    def send_own(k):
-        for q in range(SPLITS[k]):
+    def send_own(k, first=0, last=None):
+        for q in range(SPLITS[k])[first:last]:
             pl.when(has_right)(lambda q=q: z_copy(k, q, i, True, True).start())
             pl.when(has_left)(lambda q=q: z_copy(k, q, i, False, True).start())
 
@@ -228,8 +228,8 @@
             pl.when(has_left)(lambda: z_copy(k, q, s, False, False).start())
             y_copy(k, q, s, g).start()
 
-    def serve_all(k, d):
-        for q in range(SPLITS[k]):
+    def serve_all(k, d, first=0, last=None):
+        for q in range(SPLITS[k])[first:last]:
             serve(k, d, q)
 
     def each(d, f):
@@ -287,6 +287,8 @@
 
     send_own(W_IN)
     send_own(W_OUT)
+    gate_half = SPLITS[W_GATE] // 2
+    send_own(W_GATE, 0, gate_half)
     share(E_TOK, tokens, tok_at)
     share(E_GAIN, gain1, gain_at)
     for k in range(5):
@@ -296,8 +298,11 @@
     for d in range(1, n_fs):
         serve_all(W_IN, d)
         serve_all(W_OUT, d)
-    send_own(W_GATE)
+        if d == 1:
+            send_own(W_GATE, gate_half)
+            serve_all(W_GATE, 1, 0, gate_half)
     send_own(W_UP)
+    send_own(W_DOWN)
 
     take(E_TOK, tokens, tok_at)
     take(E_GAIN, gain1, gain_at)
@@ -312,6 +317,7 @@
             jnp.bfloat16
         )
 
+    serve_all(W_GATE, 1, gate_half)
     arrived(W_IN)
     pool_in = jnp.dot(x2[...], b_in[...], preferred_element_type=jnp.float32).astype(jnp.bfloat16)
     group_local = pool_w.shape[0]
@@ -338,8 +344,7 @@
     own_pool = stage.at[:, pl.ds(0, channels)]
     cols(pooled, j, channels)[...] = own_pool[...]
     share(E_POOL, own_pool, pool_at)
-    serve_all(W_GATE, 1)
-    send_own(W_DOWN)
+    serve_all(W_UP, 1, 0, 1)
     arrived(W_OUT)
     take(E_POOL, own_pool, pool_at)
     mixed[...] = tokens[...].astype(jnp.float32) + jnp.dot(
@@ -352,6 +357,7 @@
     own_sq = sq.at[n_tp]
     own_sq[...] = partial_sq
     share(E_SQ, own_sq, sq_at)
+    serve_all(W_UP, 1, 1)
     take(E_SQ, own_sq, sq_at)
     total_sq = sq[n_tp]
     for o in range(1, n_tp):
@@ -366,10 +372,14 @@
     x2_at = lambda t: cols(x2_full, t, feat)
     share(E_X2, own_x2, x2_at)
 
+    serve_all(W_DOWN, 1)
+    take(E_X2, own_x2, x2_at)
     for d in range(2, n_fs):
         serve_all(W_GATE, d)
-    take(E_X2, own_x2, x2_at)
-    serve_all(W_UP, 1)
+        if d < n_fs - 1:
+            serve_all(W_UP, d)
+            serve_all(W_DOWN, d)
+    serve_all(W_UP, n_fs - 1, 0, 1)
     arrived(W_GATE)
 
     def project(b, acc, at):
@@ -382,11 +392,11 @@
             acc[...] += jnp.dot(at[:, k_at], b[k_at, :], preferred_element_type=jnp.float32)
 
     project(b_gate, gate_acc, x2_full)
-    for d in range(2, n_fs):
-        serve_all(W_UP, d)
-    serve_all(W_DOWN, 1)
+    serve_all(W_UP, n_fs - 1, 1)
+    down_half = SPLITS[W_DOWN] // 2
+    serve_all(W_DOWN, n_fs - 1, 0, down_half)
     arrived(W_UP)
-    up_chunk = 64
+    up_chunk = 128
 
     @pl.loop(0, length // up_chunk)
     def _(r):
@@ -415,8 +425,8 @@
     own_copy(W_DOWN).wait()
     down(i)
     for d in range(1, n_fs):
-        if d > 1:
-            serve_all(W_DOWN, d)
+        if d == n_fs - 1:
+            serve_all(W_DOWN, d, down_half)
 
         def finish(s):
             wait_y(W_DOWN, s)
@@ -523,7 +533,7 @@
 
 def solution(mesh):
     n_grp, n_fs, n_tp = mesh.shape["grp"], mesh.shape["fs"], mesh.shape["tp"]
-    body = functools.partial(fused, n_fs, n_tp) if n_grp == 2 and n_fs == n_tp <= 8 else local
+    body = functools.partial(fused, n_fs, n_tp) if n_grp == 2 and 4 <= n_fs == n_tp <= 8 else local
     return jax.shard_map(
         body,
         mesh=mesh,

time: 218 us -> 201 us (0.922)
  Pallas kernels: 212 us -> 195 us
    pallas_call x1, Pallas kernels: 212 us -> 195 us  [fused(): pl.pallas_call(functools.partial(kernel, n_fs, n_tp), out_shape=jax.Shape...]
where the time goes in v2:
time: 201 us
  Pallas kernels  195 us (97%)
  local copies, waits for them, and re-layouts  5.61 us (3%)
    pallas_call x1, Pallas kernels, fused(): pl.pallas_call(functools.partial(kernel, n_fs, n_tp), out_shape=jax.Shape...  195 us

profile of v2, /device:TPU:0, one launch (start us, length us, event | category | flops | bytes accessed | tf_op | source)
XLA Modules:
  0.0 200.5 jit_solution(15643670277333584141)
XLA Ops:
  0.0 1.3 broadcast_in_dim.13.scale
  1.3 1.3 broadcast_in_dim.12.gain1
  2.6 1.3 broadcast_in_dim.14.gain2
  3.8 194.9 %shard_map.100 = bf16[384,512]{1,0:T(8,128)(2,1)} custom-call(bf16[384,512]{1,0:T(8,128)(2,1)} %bitcast.3, f32[8,512]{1,0:T(8,128)} %broadcast_in_dim.12.gain1, bf16[2,128,128]{2,1,0:T(8,128)(2,1)} %pool_w.1, f32[8,256]{1,0:T(8,128)} %broadcast_in_dim.13.scale, f32[8,512]{1,0:T(8,128)} %broadcast_in_dim.14.gain2, bf16[512,256]{1,0:T(8,128)(2,1)} %w_in.1, ...), custom_call_target="tpu_custom_call" | custom-call | tf_op jit(solution)/shard_map/pallas_call | solution.py:500
  198.8 1.8 copy.12
